TPU v7x, 32 devices: a whole 2x2x4 slice. The times are simulated.
32 devices in a mesh: fs: 8 (over z, y), tp: 4 (over x, core).
Axes of the slice: x: 2, y: 2, z: 4, core: 2. Of those that a mesh axis runs over, the one named last changes fastest.
Arguments:
- tokens: bfloat16 [16, 384, 2048], P('fs', None, 'tp'), may hold values from -34 to 34
- mix_gain: float32 [2048], replicated, may hold values from 0.1 to 1.9
- w_bgate: float32 [2048, 2048], P('fs', 'tp'), may hold values from -0.125 to 0.125
- w_cgate: float32 [2048, 2048], P('fs', 'tp'), may hold values from -0.125 to 0.125
- w_value: float32 [2048, 2048], P('fs', 'tp'), may hold values from -0.125 to 0.125
- in_scale: float32 [3, 2048], P(None, 'tp'), may hold values from 0.5 to 2
- mix_taps: float32 [3, 2048], P(None, 'tp'), may hold values from -3.5 to 3.5
- w_mixout: float32 [2048, 2048], P('tp', 'fs'), may hold values from -0.125 to 0.125
- mixout_scale: float32 [1, 2048], P(None, 'fs'), may hold values from 0.5 to 2
- ffn_gain: float32 [2048], replicated, may hold values from 0.1 to 1.9
- w_upgate: float32 [2048, 5632], P('fs', 'tp'), may hold values from -0.125 to 0.125
- w_upval: float32 [2048, 5632], P('fs', 'tp'), may hold values from -0.125 to 0.125
- up_scale: float32 [2, 5632], P(None, 'tp'), may hold values from 0.5 to 2
- ffn_taps: float32 [2, 3, 5632], P(None, None, 'tp'), may hold values from -3.5 to 3.5
- w_down: float32 [5632, 2048], P('tp', 'fs'), may hold values from -0.078125 to 0.078125
- down_scale: float32 [1, 2048], P(None, 'fs'), may hold values from 0.5 to 2
Outputs:
- layer_out: bfloat16 [16, 384, 2048], P('fs', None, 'tp')
All inputs are finite; a program needn't handle non-finite values.
Results may differ from a plain program's by a relative error of at most 0.015.
Values may be sent and summed in bfloat16 or wider, within the bound.
A program may use at most 64 MiB of HBM per device.

v0:
```python
import functools

import jax
import jax.numpy as jnp
from jax import lax
from jax.experimental import pallas as pl
from jax.experimental.pallas import tpu as pltpu
from jax.sharding import PartitionSpec as P

EPS = 1e-06
MESH = pl.DeviceIdType.MESH
F32 = jnp.float32
BF16 = jnp.bfloat16
S, A, B, C, D = range(5)


def shifted(values, by):
    rows = lax.broadcasted_iota(jnp.int32, values.shape, 0)
    return jnp.where(rows >= by, pltpu.roll(values, by, 0), 0.0)


def causal_taps(values, taps):
    return shifted(values, 2) * taps[0:1] + shifted(values, 1) * taps[1:2] + values * taps[2:3]


def layer_kernel(
    n, n_tp, seqs, tok, gain1, gain2, iscale, mtaps, uscale, ftaps, mscale, dscale,
    w_bgate, w_cgate, w_value, w_mixout, w_upgate, w_upval, w_down, out,
    buf_s, buf_a, buf_b, buf_c, buf_d, f_bgate, f_cgate, f_value, f_mixout, f_upgate, f_upval,
    f_down, xg, rg, normed, gated, active,
    parts_m, recv_m, parts_d, recv_d,
    ring_send, ring_recv, tok_send, tok_recv, mix_send, mix_recv, res_send, res_recv,
    down_send, down_recv, local_sem,
):
    fs, me = lax.axis_index("fs"), lax.axis_index("tp")
    rows, own = tok.shape
    length = rows // seqs
    bpo = n // n_tp
    bw = own // bpo
    width = own * n_tp
    bufs = (buf_s, buf_a, buf_b, buf_c, buf_d)
    hi, lo = n // 2, n - 1 - n // 2

    odd = fs % 2
    pos = (1 - odd) * (fs // 2) + odd * (n - 1 - fs // 2)

    def member(q):
        q = (q + 2 * n) % n
        back = q // (n // 2)
        return (1 - back) * (2 * q) + back * (2 * (n - 1 - q) + 1)

    def hops(h, d):
        return hi if h == d else lo

    def ring(g, h, d, k):
        sign = 1 - 2 * d
        owner = member(pos - sign * (k - 1))
        half = bufs[g].shape[1] // 2
        piece = bufs[g].at[owner, pl.ds(h * half, half)]
        return pltpu.make_async_remote_copy(
            src_ref=piece,
            dst_ref=piece,
            send_sem=ring_send.at[g, h, d, k - 1],
            recv_sem=ring_recv.at[g, h, d, k - 1],
            device_id={"fs": member(pos + sign)},
            device_id_type=MESH,
        )

    def begin(g, halves=(0, 1)):
        for h in halves:
            for d in (0, 1):
                ring(g, h, d, 1).start()

    def arrive(g, k, halves=(0, 1)):
        for h in halves:
            for d in (0, 1):
                if k <= hops(h, d):
                    ring(g, h, d, k).wait_recv()
                    if k < hops(h, d):
                        ring(g, h, d, k + 1).start()

    def to_peer(src, dst, send, recv, r):
        return pltpu.make_async_remote_copy(
            src_ref=src, dst_ref=dst, send_sem=send, recv_sem=recv,
            device_id={"tp": (me + r) % n_tp}, device_id_type=MESH,
        )

    sources = (w_bgate, w_cgate, w_value, w_mixout, w_upgate, w_upval, w_down)
    floats = (f_bgate, f_cgate, f_value, f_mixout, f_upgate, f_upval, f_down)
    loads = [
        pltpu.make_async_copy(source, held, local_sem.at[i])
        for i, (source, held) in enumerate(zip(sources, floats))
    ]
    for copy in loads:
        copy.start()

    def cast_rows(held, put):
        tile = 32

        def step(i, carry):
            at = pl.ds(pl.multiple_of(i * tile, tile), tile)
            put(at, held[at, :].astype(BF16))
            return carry

        lax.fori_loop(0, held.shape[0] // tile, step, 0)

    def put_in(i):
        def put(at, values):
            buf_a[fs, at, i * own : (i + 1) * own] = values

        return put

    def put_up(i):
        def put(at, values):
            for j in range(values.shape[1] // 128):
                to = j * 256 + i * 128
                buf_c[fs, at, to : to + 128] = values[:, j * 128 : (j + 1) * 128]

        return put

    def put_mixout(at, values):
        buf_b[fs, at, :] = values

    def put_down(at, values):
        buf_d[fs, at, :] = values

    buf_s[fs] = jnp.zeros(buf_s.shape[1:], F32)
    buf_s[fs, 0:1, :] = mscale[...]
    buf_s[fs, 1:2, :] = dscale[...]
    for i in range(3):
        loads[i].wait()
        cast_rows(floats[i], put_in(i))

    barrier = pltpu.get_barrier_semaphore()
    for sign in (1, -1):
        pl.semaphore_signal(
            barrier, inc=1, device_id={"fs": member(pos + sign)}, device_id_type=MESH
        )
    for r in range(1, n_tp):
        pl.semaphore_signal(
            barrier, inc=1, device_id={"tp": (me + r) % n_tp}, device_id_type=MESH
        )
    pl.semaphore_wait(barrier, 1 + n_tp)

    begin(S)
    begin(A)
    tok_copies = [
        to_peer(tok, xg.at[me], tok_send.at[r - 1], tok_recv.at[r - 1], r) for r in range(1, n_tp)
    ]
    for copy in tok_copies:
        copy.start()
    xg[me] = tok[...]
    for copy in loads[3:]:
        copy.wait()
    cast_rows(f_mixout, put_mixout)
    cast_rows(f_upgate, put_up(0))
    cast_rows(f_upval, put_up(1))

    def normalize(source, gain):
        tile = 32

        def step(i, carry):
            at = pl.ds(pl.multiple_of(i * tile, tile), tile)
            squares = jnp.zeros((tile, 1), F32)
            for t in range(n_tp):
                piece = source[t, at, :].astype(F32)
                squares = squares + jnp.sum(piece * piece, axis=-1, keepdims=True)
            factor = lax.rsqrt(squares * (1.0 / width) + EPS)
            for t in range(n_tp):
                cols = slice(t * own, (t + 1) * own)
                piece = source[t, at, :].astype(F32)
                normed[at, cols] = (piece * factor * gain[:, cols]).astype(BF16)
            return carry

        lax.fori_loop(0, rows // tile, step, 0)

    arrive(S, 1)
    arrive(A, 1)
    cast_rows(f_down, put_down)
    for k in range(2, hi + 1):
        arrive(S, k)
    for k in range(2, hi):
        arrive(A, k)
    begin(B)
    begin(C, (0,))
    for copy in tok_copies:
        copy.wait_recv()
    normalize(xg, gain1)
    arrive(A, hi)

    mixed = min(256, own)

    def mixer(s):
        lines = slice(s * length, (s + 1) * length)

        def step(j, carry):
            def product(i):
                at = pl.ds(pl.multiple_of(i * own + j * mixed, 128), mixed)
                matrix = buf_a[:, :, at].reshape(width, mixed)
                return jnp.dot(normed[lines, :], matrix, preferred_element_type=F32)

            at = pl.ds(pl.multiple_of(j * mixed, 128), mixed)
            scales = iscale[:, at]
            inner = (product(1) * scales[1:2]) * (product(2) * scales[2:3])
            convolved = causal_taps(inner, mtaps[:, at])
            gated[lines, at] = (product(0) * scales[0:1] * convolved).astype(BF16)
            return carry

        lax.fori_loop(0, own // mixed, step, 0)

    for s in range(seqs):
        mixer(s)
        if s == 0:
            arrive(B, 1)
    begin(C, (1,))
    for k in range(2, hi):
        arrive(B, k)
    arrive(C, 1, (0,))
    arrive(B, hi)
    arrive(C, 1, (1,))

    mix_copies = []
    for r in list(range(1, n_tp)) + [0]:
        for b in range(bpo):
            owner = (me + r) % n_tp * bpo + b
            for s in range(seqs):
                lines = slice(s * length, (s + 1) * length)
                part = jnp.dot(gated[lines, :], buf_b[owner], preferred_element_type=F32)
                parts_m[r * bpo + b, lines, :] = (part * buf_s[owner, 0:1, :]).astype(BF16)
            if r:
                copy = to_peer(
                    parts_m.at[r * bpo + b], recv_m.at[r - 1, b],
                    mix_send.at[r - 1, b], mix_recv.at[r - 1, b], r,
                )
                copy.start()
                mix_copies.append(copy)
    arrive(C, 2, (0,))

    for copy in mix_copies:
        copy.wait_recv()
    tile = 64

    def total_of(base, own_part, received, store):
        def step(i, carry):
            at = pl.ds(pl.multiple_of(i * tile, tile), tile)
            for b in range(bpo):
                cols = slice(b * bw, (b + 1) * bw)
                total = own_part(b, at).astype(F32)
                for r in range(1, n_tp):
                    total = total + received[r - 1, b, at, :].astype(F32)
                store(at, cols, (base(at, cols).astype(F32) + total).astype(BF16))
            return carry

        lax.fori_loop(0, rows // tile, step, 0)

    def store_resid(at, cols, values):
        rg[me, at, cols] = values

    total_of(lambda at, cols: tok[at, cols], lambda b, at: parts_m[b, at, :], recv_m, store_resid)
    res_copies = [
        to_peer(rg.at[me], rg.at[me], res_send.at[r - 1], res_recv.at[r - 1], r)
        for r in range(1, n_tp)
    ]
    for copy in res_copies:
        copy.start()
    arrive(C, 2, (1,))
    for k in range(3, hi):
        arrive(C, k)
    begin(D)
    for copy in res_copies:
        copy.wait_recv()
    normalize(rg, gain2)
    arrive(C, hi)

    tiles = buf_c.shape[2] // 256

    def up(s):
        lines = slice(s * length, (s + 1) * length)

        def step(j, carry):
            at = pl.ds(pl.multiple_of(j * 256, 256), 256)
            matrix = buf_c[:, :, at].reshape(width, 256)
            both = jnp.dot(normed[lines, :], matrix, preferred_element_type=F32)
            half = pl.ds(pl.multiple_of(j * 128, 128), 128)
            gate = causal_taps(both[:, :128] * uscale[0:1, half], ftaps[0, :, half])
            val = causal_taps(both[:, 128:] * uscale[1:2, half], ftaps[1, :, half])
            active[lines, half] = (gate / (1.0 + jnp.exp(-gate)) * val).astype(BF16)
            return carry

        lax.fori_loop(0, tiles, step, 0)

    for s in range(seqs):
        up(s)
        if s == 0:
            arrive(D, 1)

    def down(owner):
        t = owner // bpo
        r = (t - me + n_tp) % n_tp
        b = owner % bpo
        for s in range(seqs):
            lines = slice(s * length, (s + 1) * length)
            part = jnp.dot(active[lines, :], buf_d[owner], preferred_element_type=F32)
            parts_d[owner, lines, :] = (part * buf_s[owner, 1:2, :]).astype(BF16)

            @pl.when(r != 0)
            def _():
                pltpu.make_async_remote_copy(
                    src_ref=parts_d.at[owner, lines], dst_ref=recv_d.at[r - 1, b, lines],
                    send_sem=down_send.at[owner, s], recv_sem=down_recv.at[r - 1, b, s],
                    device_id={"tp": t}, device_id_type=MESH,
                ).start()

    arrive(D, 2)
    down(fs)
    for k in range(1, hi + 1):
        if k > 2:
            arrive(D, k)
        down(member(pos - k))
        if (2 * k) % n:
            down(member(pos + k))

    ends = []
    for r in range(1, n_tp):
        for b in range(bpo):
            owner = (me + r) % n_tp * bpo + b
            for s in range(seqs):
                lines = slice(s * length, (s + 1) * length)
                ends.append(
                    to_peer(
                        parts_d.at[owner, lines], recv_d.at[r - 1, b, lines],
                        down_send.at[owner, s], down_recv.at[r - 1, b, s], r,
                    )
                )
    for copy in ends:
        copy.wait_recv()

    def store_out(at, cols, values):
        out[at, cols] = values

    total_of(
        lambda at, cols: rg[me, at, cols], lambda b, at: parts_d[me * bpo + b, at, :], recv_d,
        store_out,
    )

    for copy in tok_copies + mix_copies + res_copies + ends:
        copy.wait_send()
    for g in range(5):
        for h in (0, 1):
            for d in (0, 1):
                for k in range(1, hops(h, d) + 1):
                    ring(g, h, d, k).wait_send()


def on_device(
    n,
    n_tp,
    tokens,
    mix_gain,
    w_bgate,
    w_cgate,
    w_value,
    in_scale,
    mix_taps,
    w_mixout,
    mixout_scale,
    ffn_gain,
    w_upgate,
    w_upval,
    up_scale,
    ffn_taps,
    w_down,
    down_scale,
):
    seqs, length, own = tokens.shape
    rows = seqs * length
    width = own * n_tp
    part = w_bgate.shape[0]
    ff = w_upgate.shape[1]
    pad = -ff % 128
    ffp = ff + pad
    bw = w_mixout.shape[1]

    if pad:
        w_upgate, w_upval, up_scale, ffn_taps = (
            jnp.pad(x, [(0, 0)] * (x.ndim - 1) + [(0, pad)])
            for x in (w_upgate, w_upval, up_scale, ffn_taps)
        )
        w_down = jnp.pad(w_down, ((0, pad), (0, 0)))
    weights = (w_bgate, w_cgate, w_value, w_mixout, w_upgate, w_upval, w_down)
    held = [(16, bw), (part, 3 * own), w_mixout.shape, (part, 2 * ffp), w_down.shape]
    bpo = n // n_tp
    hi = n // 2
    vmem, dma = pltpu.VMEM, pltpu.SemaphoreType.DMA
    result = pl.pallas_call(
        functools.partial(layer_kernel, n, n_tp, seqs),
        out_shape=jax.ShapeDtypeStruct((rows, own), BF16),
        in_specs=[pl.BlockSpec(memory_space=pltpu.VMEM)] * 9
        + [pl.BlockSpec(memory_space=pl.ANY)] * 7,
        out_specs=pl.BlockSpec(memory_space=pltpu.VMEM),
        scratch_shapes=[vmem((n, *shape), BF16 if i else F32) for i, shape in enumerate(held)]
        + [vmem(w.shape, F32) for w in weights]
        + [
            vmem((n_tp, rows, own), BF16),
            vmem((n_tp, rows, own), BF16),
            vmem((rows, width), BF16),
            vmem((rows, own), BF16),
            vmem((rows, ffp), BF16),
            vmem((n, rows, bw), BF16),
            vmem((n_tp - 1, bpo, rows, bw), BF16),
            vmem((n, rows, bw), BF16),
            vmem((n_tp - 1, bpo, rows, bw), BF16),
            dma((5, 2, 2, hi)),
            dma((5, 2, 2, hi)),
            dma((n_tp - 1,)),
            dma((n_tp - 1,)),
            dma((n_tp - 1, bpo)),
            dma((n_tp - 1, bpo)),
            dma((n_tp - 1,)),
            dma((n_tp - 1,)),
            dma((n, seqs)),
            dma((n_tp - 1, bpo, seqs)),
            dma((7,)),
        ],
        compiler_params=pltpu.CompilerParams(
            collective_id=0, has_side_effects=True, vmem_limit_bytes=67043328
        ),
        name="layer",
    )(
        tokens.reshape(rows, own), mix_gain.reshape(1, width), ffn_gain.reshape(1, width),
        in_scale, mix_taps, up_scale, ffn_taps, mixout_scale, down_scale, *weights,
    )
    return result.reshape(seqs, length, own)


def solution(mesh):
    in_specs = (
        P("fs", None, "tp"),
        P(),
        P("fs", "tp"),
        P("fs", "tp"),
        P("fs", "tp"),
        P(None, "tp"),
        P(None, "tp"),
        P("tp", "fs"),
        P(None, "fs"),
        P(),
        P("fs", "tp"),
        P("fs", "tp"),
        P(None, "tp"),
        P(None, None, "tp"),
        P("tp", "fs"),
        P(None, "fs"),
    )
    out_specs = P("fs", None, "tp")
    body = functools.partial(on_device, mesh.shape["fs"], mesh.shape["tp"])
    return jax.shard_map(body, mesh=mesh, in_specs=in_specs, out_specs=out_specs, check_vma=False)
```

profile of v0, /device:TPU:3, one launch (start us, length us, event | category | flops | bytes accessed | tf_op | source)
XLA Modules:
  0.0 279.3 jit_solution(1873455611510781969)
XLA Ops:
  0.0 1.4 copy.17.ftaps
  1.4 275.8 %layer.1 = bf16[768,512]{1,0:T(8,128)(2,1)} custom-call(bf16[768,512]{1,0:T(8,128)(2,1)} %bitcast.5, f32[1,2048]{1,0:T(1,128)} %bitcast.6, f32[1,2048]{1,0:T(1,128)} %bitcast.7, f32[3,512]{1,0:T(4,128)} %iscale.1, f32[3,512]{1,0:T(4,128)} %mtaps.1, f32[2,1408]{1,0:T(2,128)} %uscale.1, f32[2,3,1408]{2,1,0:T(4,128)} %copy.17.ftaps, f32[1,256]{1,0:T(1,128)} %mscale.1, ...), custom_call_target="tpu_custom_call" | custom-call | tf_op jit(solution)/shard_map/layer/pallas_call | solution.py:395
  277.2 2.1 copy.19
where the time goes:
time: 280 us; the launch traced here: 279 us
  Pallas kernels  276 us (99%)
  local copies, waits for them, and re-layouts  3.45 us (1%)
    pallas_call x1, Pallas kernels, on_device(): pl.pallas_call(functools.partial(layer_kernel, n, n_tp, seqs), out_shape=...  276 us

commit v1 on v0

v1 whole, which is shorter than its diff:
```python
import functools

import jax
import jax.numpy as jnp
from jax import lax
from jax.experimental import pallas as pl
from jax.experimental.pallas import tpu as pltpu
from jax.sharding import PartitionSpec as P

EPS = 1e-06
MESH = pl.DeviceIdType.MESH
F32 = jnp.float32
BF16 = jnp.bfloat16
S, A, B, C, D = range(5)
MIX, DOWN = 0, 1


def shifted(values, by):
    rows = lax.broadcasted_iota(jnp.int32, values.shape, 0)
    return jnp.where(rows >= by, pltpu.roll(values, by, 0), 0.0)


def causal_taps(values, taps):
    return shifted(values, 2) * taps[0:1] + shifted(values, 1) * taps[1:2] + values * taps[2:3]


def join_halves(first, second, which):
    half = first.shape[-1] // 2
    lanes = lax.broadcasted_iota(jnp.int32, first.shape, 1)
    low = jnp.where(lanes < half, first, pltpu.roll(second, half, 1))
    high = jnp.where(lanes < half, pltpu.roll(first, half, 1), second)
    return jnp.where(which == 0, low, high)


def layer_kernel(
    n, n_tp, tok, gain1, gain2, iscale, mtaps, uscale, ftaps, mscale, dscale,
    w_bgate, w_cgate, w_value, w_mixout, w_upgate, w_upval, w_down, out,
    buf_s, buf_a, buf_b, buf_c, buf_d, st_a, st_b, st_c, st_d,
    f_bgate, f_cgate, f_value, f_mixout, f_upgate, f_upval, f_down,
    xg, normed, gated, active, parts, zparts, recv_core, recv_x, recv_z,
    wz_send, wz_recv, wy_send, wy_recv, ag_z_send, ag_z_recv, ag_x_send, ag_x_recv,
    ag_c_send, ag_c_recv, rs_z_send, rs_z_recv, rs_x_send, rs_x_recv, rs_c_send, rs_c_recv,
    local_sem,
):
    fs, me = lax.axis_index("fs"), lax.axis_index("tp")
    seqs, length, own = tok.shape
    width = own * n_tp
    planes, chips = n // 2, n_tp // 2
    bpo = n // n_tp
    bw = own // bpo
    sub = own // 2
    y, zz = fs % 2, fs // 2
    zi = zz % 2
    other = 1 - zi
    x, c = me // 2, me % 2
    blocks = f_upgate.shape[1] // 128
    full, odd = blocks // 2, blocks % 2
    second = full + odd
    down_rows = full * 128 + odd * 64

    def plane(r):
        result, bit = 0, 1
        while bit < planes:
            digit = zz // bit % 2
            result = result + bit * ((1 - digit) if r & bit else digit)
            bit *= 2
        return result

    def tp_of(r, core):
        return (x + r) % chips * 2 + core

    def remote(src, dst, send, recv, where):
        return pltpu.make_async_remote_copy(
            src_ref=src, dst_ref=dst, send_sem=send, recv_sem=recv,
            device_id=where, device_id_type=MESH,
        )

    bufs = (buf_s, buf_a, buf_b, buf_c, buf_d)
    stages = (None, st_a, st_b, st_c, st_d)

    def piece(g, at):
        return bufs[g].at[at, pl.ds(0, down_rows)] if g == D else bufs[g].at[at]

    def to_plane(g, r):
        src = stages[g] if r % 2 and g != S else piece(g, fs)
        return remote(
            src, piece(g, fs), wz_send.at[g, r - 1], wz_recv.at[g, r - 1],
            {"fs": plane(r) * 2 + y},
        )

    def to_row(g, r):
        at = piece(g, plane(r) * 2 + y)
        return remote(at, at, wy_send.at[g, r], wy_recv.at[g, r], {"fs": fs + 1 - 2 * y})

    def launch(g, rs):
        for r in rs:
            if r:
                to_plane(g, r).start()
            else:
                to_row(g, 0).start()

    def arrive(g, rs):
        for r in rs:
            to_plane(g, r).wait_recv()
            to_row(g, r).start()

    def complete(g):
        for r in range(planes):
            to_row(g, r).wait_recv()

    across = range(1, planes)

    def ag_z(k, s, src=None):
        at = xg.at[zi, me, s]
        return remote(
            at if src is None else src, at, ag_z_send.at[k, s], ag_z_recv.at[k, s],
            {"fs": fs + 2 - 4 * zi},
        )

    def ag_x(k, s, r, i, src=None):
        at = xg.at[other if i else zi, me, s]
        return remote(
            at if src is None else src, at, ag_x_send.at[k, s, r - 1, i],
            ag_x_recv.at[k, s, r - 1, i], {"tp": tp_of(r, c)},
        )

    def ag_c(k, s, r, i, src=None):
        at = xg.at[other if i else zi, tp_of(chips - r, c), s]
        return remote(
            at if src is None else src, at, ag_c_send.at[k, s, r, i], ag_c_recv.at[k, s, r, i],
            {"tp": me + 1 - 2 * c},
        )

    def gather_own(k, s, src=None):
        ag_z(k, s, src).start()
        for r in range(1, chips):
            ag_x(k, s, r, 0, src).start()
        ag_c(k, s, 0, 0, src).start()

    def gather_z(k, s):
        ag_z(k, s).wait_recv()
        for r in range(1, chips):
            ag_x(k, s, r, 1).start()
        ag_c(k, s, 0, 1).start()

    def gather_x(k, s):
        for i in (0, 1):
            for r in range(1, chips):
                ag_x(k, s, r, i).wait_recv()
                ag_c(k, s, r, i).start()

    def gather_done(k, s):
        for i in (0, 1):
            for r in range(chips):
                ag_c(k, s, r, i).wait_recv()

    def gather_sent(k, src=None):
        for s in range(seqs):
            ag_z(k, s).wait_send()
            for i in (0, 1):
                for r in range(1, chips):
                    ag_x(k, s, r, i).wait_send()
                for r in range(chips):
                    ag_c(k, s, r, i).wait_send()

    def rs_c(k, s, r):
        return remote(
            parts.at[r, 1, s], recv_core.at[k, r, s], rs_c_send.at[k, s, r],
            rs_c_recv.at[k, s, r], {"tp": me + 1 - 2 * c},
        )

    def rs_x(k, s, r):
        return remote(
            parts.at[r, 0, s], recv_x.at[k, r - 1, s], rs_x_send.at[k, s, r - 1],
            rs_x_recv.at[k, s, r - 1], {"tp": tp_of(r, c)},
        )

    def rs_z(k, s):
        return remote(
            zparts.at[s], recv_z.at[k, s], rs_z_send.at[k, s], rs_z_recv.at[k, s],
            {"fs": fs + 2 - 4 * zi},
        )

    def products(k, s, r, side):
        owner = tp_of(r, 1 - c if side else c)
        source, held = ((gated, buf_b), (active, buf_d))[k]
        for i in (0, 1):
            for b in range(bpo):
                at = owner * bpo + b
                part = jnp.dot(source[s, i], held[at], preferred_element_type=F32)
                parts[r, side, s, i, :, b * bw : (b + 1) * bw] = (
                    part * buf_s[at, k : k + 1, :]
                ).astype(BF16)

    order = list(range(1, chips)) + [0]
    tile = 64

    def scatter_begin(k, s):
        for r in order:
            products(k, s, r, 1)
            rs_c(k, s, r).start()
        for r in order:
            products(k, s, r, 0)

    def scatter_x(k, s):
        for r in range(1, chips):
            rs_c(k, s, r).wait_recv()

            def step(j, carry, r=r):
                at = pl.ds(pl.multiple_of(j * tile, tile), tile)
                for i in (0, 1):
                    total = parts[r, 0, s, i, at, :].astype(F32)
                    total = total + recv_core[k, r, s, i, at, :].astype(F32)
                    parts[r, 0, s, i, at, :] = total.astype(BF16)
                return carry

            lax.fori_loop(0, length // tile, step, 0)
            rs_x(k, s, r).start()

    def quad(k, s, i, at):
        total = parts[0, 0, s, i, at, :].astype(F32) + recv_core[k, 0, s, i, at, :].astype(F32)
        for r in range(1, chips):
            total = total + recv_x[k, r - 1, s, i, at, :].astype(F32)
        return total

    def scatter_z(k, s):
        rs_c(k, s, 0).wait_recv()
        for r in range(1, chips):
            rs_x(k, s, r).wait_recv()

        def step(j, carry):
            at = pl.ds(pl.multiple_of(j * tile, tile), tile)
            zparts[s, at, :] = quad(k, s, other, at).astype(BF16)
            return carry

        lax.fori_loop(0, length // tile, step, 0)
        rs_z(k, s).start()

    def scatter_end(k, s, base, store):
        rs_z(k, s).wait_recv()

        def step(j, carry):
            at = pl.ds(pl.multiple_of(j * tile, tile), tile)
            total = quad(k, s, zi, at) + recv_z[k, s, at, :].astype(F32)
            store(at, (base(at).astype(F32) + total).astype(BF16))
            return carry

        lax.fori_loop(0, length // tile, step, 0)

    def scatter_sent(k):
        for s in range(seqs):
            for r in range(chips):
                rs_c(k, s, r).wait_send()
                if r:
                    rs_x(k, s, r).wait_send()
            rs_z(k, s).wait_send()

    barrier = pltpu.get_barrier_semaphore()
    peers = [{"fs": plane(r) * 2 + y} for r in across]
    peers += [{"fs": fs + 1 - 2 * y}, {"tp": me + 1 - 2 * c}]
    peers += [{"tp": tp_of(r, c)} for r in range(1, chips)]
    for peer in peers:
        pl.semaphore_signal(barrier, inc=1, device_id=peer, device_id_type=MESH)

    sources = (w_bgate, w_cgate, w_value, w_mixout, w_upgate, w_upval, w_down)
    floats = (f_bgate, f_cgate, f_value, f_mixout, f_upgate, f_upval, f_down)
    loads = [
        pltpu.make_async_copy(source, held, local_sem.at[i])
        for i, (source, held) in enumerate(zip(sources, floats))
    ]
    for copy in loads:
        copy.start()

    def cast_rows(rows, put):
        step_rows = 32

        def step(i, carry):
            put(i * step_rows, step_rows)
            return carry

        lax.fori_loop(0, rows // step_rows, step, 0)

    def rows_at(start, count):
        return pl.ds(pl.multiple_of(start, 32), count)

    def lanes_at(start, count):
        return pl.ds(pl.multiple_of(start, 128), count)

    def put_in(start, count):
        at = rows_at(start, count)
        for i, held in enumerate((f_bgate, f_cgate, f_value)):
            cols = slice(i * sub, (i + 1) * sub)
            buf_a[fs, at, cols] = held[at, lanes_at(zi * sub, sub)].astype(BF16)
            st_a[at, cols] = held[at, lanes_at(other * sub, sub)].astype(BF16)

    def put_mixout(start, count):
        at = rows_at(start, count)
        buf_b[fs, at, :] = f_mixout[rows_at(zi * sub + start, count), :].astype(BF16)
        st_b[at, :] = f_mixout[rows_at(other * sub + start, count), :].astype(BF16)

    def put_up(start, count):
        at = rows_at(start, count)
        for j in range(full):
            for i, held in enumerate((f_upgate, f_upval)):
                cols = slice(j * 256 + i * 128, j * 256 + i * 128 + 128)
                mine = lanes_at((zi * second + j) * 128, 128)
                theirs = lanes_at((other * second + j) * 128, 128)
                buf_c[fs, at, cols] = held[at, mine].astype(BF16)
                st_c[at, cols] = held[at, theirs].astype(BF16)
        if odd:
            mid = slice(full * 128, full * 128 + 128)
            cols = slice(full * 256, full * 256 + 128)
            gate, val = f_upgate[at, mid], f_upval[at, mid]
            buf_c[fs, at, cols] = join_halves(gate, val, zi).astype(BF16)
            st_c[at, cols] = join_halves(gate, val, other).astype(BF16)

    def put_down(start, count):
        at = rows_at(start, count)
        buf_d[fs, at, :] = f_down[rows_at(zi * second * 128 + start, count), :].astype(BF16)
        st_d[at, :] = f_down[rows_at(other * second * 128 + start, count), :].astype(BF16)

    def put_down_mid(start, count):
        base = full * 128
        at = rows_at(base + start, count)
        buf_d[fs, at, :] = f_down[rows_at(base + zi * 64 + start, count), :].astype(BF16)
        st_d[at, :] = f_down[rows_at(base + other * 64 + start, count), :].astype(BF16)

    buf_s[fs] = jnp.zeros(buf_s.shape[1:], F32)
    buf_s[fs, 0:1, :] = mscale[...]
    buf_s[fs, 1:2, :] = dscale[...]
    for i in range(3):
        loads[i].wait()
    cast_rows(f_bgate.shape[0], put_in)
    pl.semaphore_wait(barrier, len(peers))

    launch(S, range(planes))
    gather_own(MIX, 0, tok.at[0])
    launch(A, [0] + list(across))
    for s in range(1, seqs):
        gather_own(MIX, s, tok.at[s])
    xg[zi, me] = tok[...]
    loads[3].wait()
    cast_rows(sub, put_mixout)
    launch(B, [0] + list(across))
    for i in (4, 5, 6):
        loads[i].wait()
    cast_rows(f_upgate.shape[0], put_up)
    cast_rows(full * 128, put_down)
    if odd:
        cast_rows(64, put_down_mid)
        for at in range(n):
            buf_d[at, down_rows:, :] = jnp.zeros((64, bw), BF16)

    def normalize(s, gain):
        step_rows = 32

        def step(j, carry):
            at = pl.ds(pl.multiple_of(j * step_rows, step_rows), step_rows)
            for i in (0, 1):
                squares = jnp.zeros((step_rows, 1), F32)
                for t in range(n_tp):
                    values = xg[i, t, s, at, :].astype(F32)
                    squares = squares + jnp.sum(values * values, axis=-1, keepdims=True)
                factor = lax.rsqrt(squares * (1.0 / width) + EPS)
                for t in range(n_tp):
                    cols = slice(t * own, (t + 1) * own)
                    values = xg[i, t, s, at, :].astype(F32)
                    normed[s, i, at, cols] = (values * factor * gain[:, cols]).astype(BF16)
            return carry

        lax.fori_loop(0, length // step_rows, step, 0)

    arrive(S, across)
    gather_z(MIX, 0)
    arrive(A, [1])
    for s in range(1, seqs):
        gather_z(MIX, s)
    gather_x(MIX, 0)
    for r in across:
        if r > 1:
            arrive(A, [r])
    for s in range(1, seqs):
        gather_x(MIX, s)
    launch(C, [0, 1])
    arrive(B, across)
    for s in range(seqs):
        gather_done(MIX, s)
        normalize(s, gain1)
    complete(S)
    complete(A)

    mixed = min(256, sub)

    def mixer(s):
        def step(j, carry):
            i, at = j % 2, j // 2 * mixed

            def product(m):
                cols = pl.ds(pl.multiple_of(m * sub + at, 128), mixed)
                matrix = buf_a[:, :, cols].reshape(width, mixed)
                return jnp.dot(normed[s, i], matrix, preferred_element_type=F32)

            here = pl.ds(pl.multiple_of(zi * sub + at, 128), mixed)
            scales = iscale[:, here]
            inner = (product(1) * scales[1:2]) * (product(2) * scales[2:3])
            convolved = causal_taps(inner, mtaps[:, here])
            cols = pl.ds(pl.multiple_of(at, 128), mixed)
            gated[s, i, :, cols] = (product(0) * scales[0:1] * convolved).astype(BF16)
            return carry

        lax.fori_loop(0, 2 * (sub // mixed), step, 0)

    mixer(0)
    if planes > 2:
        launch(C, [2])
    for s in range(1, seqs):
        mixer(s)
    gather_sent(MIX)
    complete(B)
    for s in range(seqs):
        scatter_begin(MIX, s)
        scatter_x(MIX, s)
    arrive(C, [1])
    launch(C, range(3, planes))
    launch(D, [0])

    for s in range(seqs):
        scatter_z(MIX, s)
    for s in range(seqs):

        def store_resid(at, values, s=s):
            xg[zi, me, s, at, :] = values

        scatter_end(MIX, s, lambda at, s=s: tok[s, at, :], store_resid)
        gather_own(DOWN, s)
    for s in range(seqs):
        gather_z(DOWN, s)
    launch(D, across)
    for s in range(seqs):
        gather_x(DOWN, s)
    for r in across:
        if r > 1:
            arrive(C, [r])
    for s in range(seqs):
        gather_done(DOWN, s)
        normalize(s, gain2)
    complete(C)

    def up(s):
        def activate(gate, val):
            return gate / (1.0 + jnp.exp(-gate)) * val

        def step(j, carry):
            i, t = j % 2, j // 2
            matrix = buf_c[:, :, lanes_at(t * 256, 256)].reshape(width, 256)
            both = jnp.dot(normed[s, i], matrix, preferred_element_type=F32)
            here = lanes_at((zi * second + t) * 128, 128)
            gate = causal_taps(both[:, :128] * uscale[0:1, here], ftaps[0, :, here])
            val = causal_taps(both[:, 128:] * uscale[1:2, here], ftaps[1, :, here])
            active[s, i, :, lanes_at(t * 128, 128)] = activate(gate, val).astype(BF16)
            return carry

        lax.fori_loop(0, 2 * full, step, 0)
        if odd:
            mid = slice(full * 128, full * 128 + 128)
            scale = join_halves(uscale[0:1, mid], uscale[1:2, mid], zi)
            taps = join_halves(ftaps[0, :, mid], ftaps[1, :, mid], zi)

            def last(i, carry):
                matrix = buf_c[:, :, full * 256 :].reshape(width, 128)
                both = jnp.dot(normed[s, i], matrix, preferred_element_type=F32)
                gate = causal_taps(both * scale, taps)
                values = activate(gate, pltpu.roll(gate, 64, 1))
                lanes = lax.broadcasted_iota(jnp.int32, values.shape, 1)
                active[s, i, :, mid] = jnp.where(lanes < 64, values, 0.0).astype(BF16)
                return carry

            lax.fori_loop(0, 2, last, 0)

    for s in range(seqs):
        up(s)
        if s == 0:
            arrive(D, across)
    scatter_sent(MIX)
    complete(D)

    for s in range(seqs):
        scatter_begin(DOWN, s)
        scatter_x(DOWN, s)
    for s in range(seqs):
        scatter_z(DOWN, s)
    for s in range(seqs):

        def store_out(at, values, s=s):
            out[s, at, :] = values

        scatter_end(DOWN, s, lambda at, s=s: xg[zi, me, s, at, :], store_out)

    gather_sent(DOWN)
    scatter_sent(DOWN)
    for g in range(5):
        for r in range(planes):
            to_row(g, r).wait_send()
            if r:
                to_plane(g, r).wait_send()


def on_device(
    n,
    n_tp,
    tokens,
    mix_gain,
    w_bgate,
    w_cgate,
    w_value,
    in_scale,
    mix_taps,
    w_mixout,
    mixout_scale,
    ffn_gain,
    w_upgate,
    w_upval,
    up_scale,
    ffn_taps,
    w_down,
    down_scale,
):
    seqs, length, own = tokens.shape
    width = own * n_tp
    part = w_bgate.shape[0]
    ff = w_upgate.shape[1]
    pad = -ff % 128
    ffp = ff + pad
    bw = w_mixout.shape[1]

    if pad:
        w_upgate, w_upval, up_scale, ffn_taps = (
            jnp.pad(x, [(0, 0)] * (x.ndim - 1) + [(0, pad)])
            for x in (w_upgate, w_upval, up_scale, ffn_taps)
        )
        w_down = jnp.pad(w_down, ((0, pad), (0, 0)))
    weights = (w_bgate, w_cgate, w_value, w_mixout, w_upgate, w_upval, w_down)
    planes, chips, sub = n // 2, n_tp // 2, own // 2
    full, odd = ffp // 128 // 2, ffp // 128 % 2
    hidden, down_rows = (full + odd) * 128, full * 128 + odd * 64
    vmem, dma = pltpu.VMEM, pltpu.SemaphoreType.DMA
    result = pl.pallas_call(
        functools.partial(layer_kernel, n, n_tp),
        out_shape=jax.ShapeDtypeStruct((seqs, length, own), BF16),
        in_specs=[pl.BlockSpec(memory_space=pltpu.VMEM)] * 9
        + [pl.BlockSpec(memory_space=pl.ANY)] * 7,
        out_specs=pl.BlockSpec(memory_space=pltpu.VMEM),
        scratch_shapes=[
            vmem((n, 8, bw), F32),
            vmem((n, part, 3 * sub), BF16),
            vmem((n, sub, bw), BF16),
            vmem((n, part, ffp), BF16),
            vmem((n, hidden, bw), BF16),
            vmem((part, 3 * sub), BF16),
            vmem((sub, bw), BF16),
            vmem((part, ffp), BF16),
            vmem((down_rows, bw), BF16),
        ]
        + [vmem(w.shape, F32) for w in weights]
        + [
            vmem((2, n_tp, seqs, length, own), BF16),
            vmem((seqs, 2, length, width), BF16),
            vmem((seqs, 2, length, sub), BF16),
            vmem((seqs, 2, length, hidden), BF16),
            vmem((chips, 2, seqs, 2, length, own), BF16),
            vmem((seqs, length, own), BF16),
            vmem((2, chips, seqs, 2, length, own), BF16),
            vmem((2, chips - 1, seqs, 2, length, own), BF16),
            vmem((2, seqs, length, own), BF16),
            dma((5, planes - 1)),
            dma((5, planes - 1)),
            dma((5, planes)),
            dma((5, planes)),
            dma((2, seqs)),
            dma((2, seqs)),
            dma((2, seqs, chips - 1, 2)),
            dma((2, seqs, chips - 1, 2)),
            dma((2, seqs, chips, 2)),
            dma((2, seqs, chips, 2)),
            dma((2, seqs)),
            dma((2, seqs)),
            dma((2, seqs, chips - 1)),
            dma((2, seqs, chips - 1)),
            dma((2, seqs, chips)),
            dma((2, seqs, chips)),
            dma((7,)),
        ],
        compiler_params=pltpu.CompilerParams(
            collective_id=0, has_side_effects=True, vmem_limit_bytes=67043328
        ),
        name="layer",
    )(
        tokens, mix_gain.reshape(1, width), ffn_gain.reshape(1, width),
        in_scale, mix_taps, up_scale, ffn_taps, mixout_scale, down_scale, *weights,
    )
    return result


def solution(mesh):
    in_specs = (
        P("fs", None, "tp"),
        P(),
        P("fs", "tp"),
        P("fs", "tp"),
        P("fs", "tp"),
        P(None, "tp"),
        P(None, "tp"),
        P("tp", "fs"),
        P(None, "fs"),
        P(),
        P("fs", "tp"),
        P("fs", "tp"),
        P(None, "tp"),
        P(None, None, "tp"),
        P("tp", "fs"),
        P(None, "fs"),
    )
    out_specs = P("fs", None, "tp")
    body = functools.partial(on_device, mesh.shape["fs"], mesh.shape["tp"])
    return jax.shard_map(body, mesh=mesh, in_specs=in_specs, out_specs=out_specs, check_vma=False)
```

time: 280 us -> 293 us (1.046); the launches traced: 279 us -> 289 us
  Pallas kernels: 276 us -> 286 us
    pallas_call x1, Pallas kernels: 276 us -> 286 us  [on_device(): pl.pallas_call(functools.partial(layer_kernel, n, n_tp), out_shape=jax.Sh...]
where the time goes in v1:
time: 293 us; the launch traced here: 289 us
  Pallas kernels  286 us (98%)
  local copies, waits for them, and re-layouts  3.45 us (1%)
    pallas_call x1, Pallas kernels, on_device(): pl.pallas_call(functools.partial(layer_kernel, n, n_tp), out_shape=jax.Sh...  286 us

profile of v1, /device:TPU:3, one launch (start us, length us, event | category | flops | bytes accessed | tf_op | source)
XLA Modules:
  0.0 289.0 jit_solution(6886676858954626901)
XLA Ops:
  0.0 1.4 copy.17.ftaps
  1.4 285.5 %layer.1 = bf16[2,384,512]{2,1,0:T(8,128)(2,1)} custom-call(bf16[2,384,512]{2,1,0:T(8,128)(2,1)} %tok.1, f32[1,2048]{1,0:T(1,128)} %bitcast.2, f32[1,2048]{1,0:T(1,128)} %bitcast.3, f32[3,512]{1,0:T(4,128)} %iscale.1, f32[3,512]{1,0:T(4,128)} %mtaps.1, f32[2,1408]{1,0:T(2,128)} %uscale.1, f32[2,3,1408]{2,1,0:T(4,128)} %copy.17.ftaps, f32[1,256]{1,0:T(1,128)} %mscale.1, ...), custom_call_target="tpu_custom_call" | custom-call | tf_op jit(solution)/shard_map/layer/pallas_call | solution.py:547
  286.9 2.1 copy.19

commit v2 on v1

--- a/solution.py
+++ b/solution.py
@@ -11,7 +11,7 @@
 MESH = pl.DeviceIdType.MESH
 F32 = jnp.float32
 BF16 = jnp.bfloat16
-S, A, B, C, D = range(5)
+S, A, F, B, C, E, D, G = range(8)
 MIX, DOWN = 0, 1
 
 
@@ -75,14 +75,22 @@
             device_id=where, device_id_type=MESH,
         )
 
-    bufs = (buf_s, buf_a, buf_b, buf_c, buf_d)
-    stages = (None, st_a, st_b, st_c, st_d)
+    bufs = (buf_s, buf_a, buf_a, buf_b, buf_c, buf_c, buf_d, buf_d)
+    stages = (None, st_a, st_a, st_b, st_c, st_c, st_d, st_d)
+    half = buf_c.shape[1] // 2
+    low, high = pl.ds(0, half), pl.ds(half, half)
+    spans = {A: low, F: high, C: low, E: high}
+    spans[D] = pl.ds(0, down_rows // 2)
+    spans[G] = pl.ds(down_rows // 2, down_rows // 2)
 
     def piece(g, at):
-        return bufs[g].at[at, pl.ds(0, down_rows)] if g == D else bufs[g].at[at]
+        return bufs[g].at[at, spans[g]] if g in spans else bufs[g].at[at]
+
+    def stage(g):
+        return stages[g].at[spans[g]] if g in spans else stages[g]
 
     def to_plane(g, r):
-        src = stages[g] if r % 2 and g != S else piece(g, fs)
+        src = stage(g) if r % 2 and g != S else piece(g, fs)
         return remote(
             src, piece(g, fs), wz_send.at[g, r - 1], wz_recv.at[g, r - 1],
             {"fs": plane(r) * 2 + y},
@@ -109,6 +117,7 @@
             to_row(g, r).wait_recv()
 
     across = range(1, planes)
+    rest = list(across)[:0:-1]
 
     def ag_z(k, s, src=None):
         at = xg.at[zi, me, s]
@@ -154,9 +163,10 @@
             for r in range(chips):
                 ag_c(k, s, r, i).wait_recv()
 
-    def gather_sent(k, src=None):
+    def gather_sent(k):
         for s in range(seqs):
-            ag_z(k, s).wait_send()
+            if k == MIX:
+                ag_z(k, s).wait_send()
             for i in (0, 1):
                 for r in range(1, chips):
                     ag_x(k, s, r, i).wait_send()
@@ -176,9 +186,11 @@
         )
 
     def rs_z(k, s):
+        src, dst = zparts.at[s], recv_z.at[k, s]
+        if k == DOWN:
+            src, dst = zparts.at[s, other], recv_z.at[k, s, 0]
         return remote(
-            zparts.at[s], recv_z.at[k, s], rs_z_send.at[k, s], rs_z_recv.at[k, s],
-            {"fs": fs + 2 - 4 * zi},
+            src, dst, rs_z_send.at[k, s], rs_z_recv.at[k, s], {"fs": fs + 2 - 4 * zi},
         )
 
     def products(k, s, r, side):
@@ -195,12 +207,40 @@
     order = list(range(1, chips)) + [0]
     tile = 64
 
-    def scatter_begin(k, s):
-        for r in order:
+    def scatter_begin(k, s, rs):
+        for r in rs:
             products(k, s, r, 1)
             rs_c(k, s, r).start()
-        for r in order:
+        for r in rs:
             products(k, s, r, 0)
+
+    def away(r):
+        return plane(r) // 2 != x
+
+    def each_down(test, do):
+        for r in [0, 1] + rest:
+
+            @pl.when(test(r))
+            def _(r=r):
+                for g in (D, G):
+                    do(g, r)
+
+    def down_launch(first):
+        @pl.when(away(0) == first)
+        def _():
+            for r in [0, 1] + rest:
+                launch(D, [r])
+                launch(G, [r])
+
+    def down_arrive(first):
+        def do(g, r):
+            if r:
+                arrive(g, [r])
+
+        each_down(lambda r: away(r) == first, do)
+
+    def down_complete(first):
+        each_down(lambda r: away(r) == first, lambda g, r: to_row(g, r).wait_recv())
 
     def scatter_x(k, s):
         for r in range(1, chips):
@@ -230,19 +270,36 @@
 
         def step(j, carry):
             at = pl.ds(pl.multiple_of(j * tile, tile), tile)
-            zparts[s, at, :] = quad(k, s, other, at).astype(BF16)
+            for i in (0, 1) if k == MIX else (other,):
+                zparts[s, i, at, :] = quad(k, s, i, at).astype(BF16)
             return carry
 
         lax.fori_loop(0, length // tile, step, 0)
         rs_z(k, s).start()
 
-    def scatter_end(k, s, base, store):
-        rs_z(k, s).wait_recv()
+    def resid(s):
+        rs_z(MIX, s).wait_recv()
 
         def step(j, carry):
             at = pl.ds(pl.multiple_of(j * tile, tile), tile)
-            total = quad(k, s, zi, at) + recv_z[k, s, at, :].astype(F32)
-            store(at, (base(at).astype(F32) + total).astype(BF16))
+            for i in (0, 1):
+                total = zparts[s, i, at, :].astype(F32) + recv_z[MIX, s, i, at, :].astype(F32)
+                xg[i, me, s, at, :] = (xg[i, me, s, at, :].astype(F32) + total).astype(BF16)
+            return carry
+
+        lax.fori_loop(0, length // tile, step, 0)
+        for i in (0, 1):
+            for r in range(1, chips):
+                ag_x(DOWN, s, r, i).start()
+            ag_c(DOWN, s, 0, i).start()
+
+    def finish(s):
+        rs_z(DOWN, s).wait_recv()
+
+        def step(j, carry):
+            at = pl.ds(pl.multiple_of(j * tile, tile), tile)
+            total = quad(DOWN, s, zi, at) + recv_z[DOWN, s, 0, at, :].astype(F32)
+            out[s, at, :] = (xg[zi, me, s, at, :].astype(F32) + total).astype(BF16)
             return carry
 
         lax.fori_loop(0, length // tile, step, 0)
@@ -335,13 +392,18 @@
 
     launch(S, range(planes))
     gather_own(MIX, 0, tok.at[0])
-    launch(A, [0] + list(across))
+    for g in (A, F):
+        launch(g, [0, 1])
     for s in range(1, seqs):
         gather_own(MIX, s, tok.at[s])
+    for r in rest:
+        launch(A, [r])
+        launch(F, [r])
     xg[zi, me] = tok[...]
     loads[3].wait()
     cast_rows(sub, put_mixout)
-    launch(B, [0] + list(across))
+    launch(B, [0, 1])
+    launch(B, rest)
     for i in (4, 5, 6):
         loads[i].wait()
     cast_rows(f_upgate.shape[0], put_up)
@@ -372,22 +434,31 @@
 
     arrive(S, across)
     gather_z(MIX, 0)
+    arrive(A, rest[:1])
     arrive(A, [1])
+    gather_x(MIX, 0)
+    arrive(F, rest[:1])
+    arrive(F, [1])
+    arrive(A, rest[1:])
+    arrive(F, rest[1:])
     for s in range(1, seqs):
         gather_z(MIX, s)
-    gather_x(MIX, 0)
-    for r in across:
-        if r > 1:
-            arrive(A, [r])
+    gather_done(MIX, 0)
+    normalize(0, gain1)
+    launch(C, [1])
+    arrive(B, across)
     for s in range(1, seqs):
         gather_x(MIX, s)
-    launch(C, [0, 1])
-    arrive(B, across)
-    for s in range(seqs):
         gather_done(MIX, s)
         normalize(s, gain1)
+    launch(E, [1])
+    for r in rest:
+        launch(C, [r])
+        launch(E, [r])
+    launch(C, [0])
     complete(S)
     complete(A)
+    complete(F)
 
     mixed = min(256, sub)
 
@@ -410,41 +481,33 @@
 
         lax.fori_loop(0, 2 * (sub // mixed), step, 0)
 
-    mixer(0)
-    if planes > 2:
-        launch(C, [2])
-    for s in range(1, seqs):
+    for s in range(seqs):
         mixer(s)
     gather_sent(MIX)
+    arrive(C, [1])
+    launch(E, [0])
     complete(B)
     for s in range(seqs):
-        scatter_begin(MIX, s)
+        scatter_begin(MIX, s, order)
         scatter_x(MIX, s)
-    arrive(C, [1])
-    launch(C, range(3, planes))
-    launch(D, [0])
-
-    for s in range(seqs):
+    arrive(E, [1])
+    arrive(C, rest[:1])
+    scatter_z(MIX, 0)
+    arrive(E, rest[:1])
+    arrive(C, rest[1:])
+    for s in range(1, seqs):
         scatter_z(MIX, s)
-    for s in range(seqs):
-
-        def store_resid(at, values, s=s):
-            xg[zi, me, s, at, :] = values
-
-        scatter_end(MIX, s, lambda at, s=s: tok[s, at, :], store_resid)
-        gather_own(DOWN, s)
-    for s in range(seqs):
-        gather_z(DOWN, s)
-    launch(D, across)
-    for s in range(seqs):
-        gather_x(DOWN, s)
-    for r in across:
-        if r > 1:
-            arrive(C, [r])
-    for s in range(seqs):
-        gather_done(DOWN, s)
-        normalize(s, gain2)
+    resid(0)
+    arrive(E, rest[1:])
+    gather_x(DOWN, 0)
+    down_launch(True)
+    for s in range(1, seqs):
+        resid(s)
+    down_launch(False)
+    gather_done(DOWN, 0)
+    normalize(0, gain2)
     complete(C)
+    complete(E)
 
     def up(s):
         def activate(gate, val):
@@ -477,28 +540,31 @@
 
             lax.fori_loop(0, 2, last, 0)
 
+    up(0)
+    down_arrive(True)
+    for s in range(1, seqs):
+        gather_x(DOWN, s)
+        gather_done(DOWN, s)
+        normalize(s, gain2)
+    down_arrive(False)
+    scatter_sent(MIX)
+    down_complete(True)
     for s in range(seqs):
-        up(s)
-        if s == 0:
-            arrive(D, across)
-    scatter_sent(MIX)
-    complete(D)
-
+        if s:
+            up(s)
+        scatter_begin(DOWN, s, order[:-1])
+        scatter_x(DOWN, s)
+    down_complete(False)
     for s in range(seqs):
-        scatter_begin(DOWN, s)
-        scatter_x(DOWN, s)
+        scatter_begin(DOWN, s, [0])
     for s in range(seqs):
         scatter_z(DOWN, s)
     for s in range(seqs):
-
-        def store_out(at, values, s=s):
-            out[s, at, :] = values
-
-        scatter_end(DOWN, s, lambda at, s=s: xg[zi, me, s, at, :], store_out)
+        finish(s)
 
     gather_sent(DOWN)
     scatter_sent(DOWN)
-    for g in range(5):
+    for g in range(8):
         for r in range(planes):
             to_row(g, r).wait_send()
             if r:
@@ -568,14 +634,14 @@
             vmem((seqs, 2, length, sub), BF16),
             vmem((seqs, 2, length, hidden), BF16),
             vmem((chips, 2, seqs, 2, length, own), BF16),
-            vmem((seqs, length, own), BF16),
+            vmem((seqs, 2, length, own), BF16),
             vmem((2, chips, seqs, 2, length, own), BF16),
             vmem((2, chips - 1, seqs, 2, length, own), BF16),
-            vmem((2, seqs, length, own), BF16),
-            dma((5, planes - 1)),
-            dma((5, planes - 1)),
-            dma((5, planes)),
-            dma((5, planes)),
+            vmem((2, seqs, 2, length, own), BF16),
+            dma((8, planes - 1)),
+            dma((8, planes - 1)),
+            dma((8, planes)),
+            dma((8, planes)),
             dma((2, seqs)),
             dma((2, seqs)),
             dma((2, seqs, chips - 1, 2)),

time: 293 us -> 234 us (0.80)
  Pallas kernels: 286 us -> 229 us
    pallas_call x1, Pallas kernels: 286 us -> 229 us  [on_device(): pl.pallas_call(functools.partial(layer_kernel, n, n_tp), out_shape=jax.Sh...]
where the time goes in v2:
time: 234 us; the launch traced here: 232 us
  Pallas kernels  229 us (98%)
  local copies, waits for them, and re-layouts  3.45 us (1%)
    pallas_call x1, Pallas kernels, on_device(): pl.pallas_call(functools.partial(layer_kernel, n, n_tp), out_shape=jax.Sh...  229 us

profile of v2, /device:TPU:3, one launch (start us, length us, event | category | flops | bytes accessed | tf_op | source)
XLA Modules:
  0.0 232.2 jit_solution(406352983202605909)
XLA Ops:
  0.0 1.4 copy.17.ftaps
  1.4 228.8 %layer.1 = bf16[2,384,512]{2,1,0:T(8,128)(2,1)} custom-call(bf16[2,384,512]{2,1,0:T(8,128)(2,1)} %tok.1, f32[1,2048]{1,0:T(1,128)} %bitcast.2, f32[1,2048]{1,0:T(1,128)} %bitcast.3, f32[3,512]{1,0:T(4,128)} %iscale.1, f32[3,512]{1,0:T(4,128)} %mtaps.1, f32[2,1408]{1,0:T(2,128)} %uscale.1, f32[2,3,1408]{2,1,0:T(4,128)} %copy.17.ftaps, f32[1,256]{1,0:T(1,128)} %mscale.1, ...), custom_call_target="tpu_custom_call" | custom-call | tf_op jit(solution)/shard_map/layer/pallas_call | solution.py:613
  230.2 2.1 copy.19

commit v3 on v2

--- a/solution.py
+++ b/solution.py
@@ -39,7 +39,7 @@
     f_bgate, f_cgate, f_value, f_mixout, f_upgate, f_upval, f_down,
     xg, normed, gated, active, parts, zparts, recv_core, recv_x, recv_z,
     wz_send, wz_recv, wy_send, wy_recv, ag_z_send, ag_z_recv, ag_x_send, ag_x_recv,
-    ag_c_send, ag_c_recv, rs_z_send, rs_z_recv, rs_x_send, rs_x_recv, rs_c_send, rs_c_recv,
+    ag_c_send, ag_c_recv, rs_z_send, rs_z_recv, rs_zz_send, rs_zz_recv, rs_x_send, rs_x_recv, rs_c_send, rs_c_recv,
     local_sem,
 ):
     fs, me = lax.axis_index("fs"), lax.axis_index("tp")
@@ -51,6 +51,7 @@
     sub = own // 2
     y, zz = fs % 2, fs // 2
     zi = zz % 2
+    inner = (zz + zz // 2) % 2
     other = 1 - zi
     x, c = me // 2, me % 2
     blocks = f_upgate.shape[1] // 128
@@ -186,7 +187,7 @@
         )
 
     def rs_z(k, s):
-        src, dst = zparts.at[s], recv_z.at[k, s]
+        src, dst = zparts.at[s, pl.ds(0, 2)], recv_z.at[k, s, pl.ds(0, 2)]
         if k == DOWN:
             src, dst = zparts.at[s, other], recv_z.at[k, s, 0]
         return remote(
@@ -217,8 +218,8 @@
     def away(r):
         return plane(r) // 2 != x
 
-    def each_down(test, do):
-        for r in [0, 1] + rest:
+    def each_down(test, do, rs):
+        for r in rs:
 
             @pl.when(test(r))
             def _(r=r):
@@ -228,19 +229,26 @@
     def down_launch(first):
         @pl.when(away(0) == first)
         def _():
-            for r in [0, 1] + rest:
+            for r in [0, 1]:
                 launch(D, [r])
                 launch(G, [r])
 
-    def down_arrive(first):
-        def do(g, r):
-            if r:
-                arrive(g, [r])
-
-        each_down(lambda r: away(r) == first, do)
+            @pl.when(inner == 0)
+            def _():
+                down_across(rest)
+
+    def down_across(rs):
+        for r in rs:
+            launch(D, [r])
+            launch(G, [r])
+
+    def down_arrive(first, rs):
+        each_down(lambda r: away(r) == first, lambda g, r: arrive(g, [r]), rs)
 
     def down_complete(first):
-        each_down(lambda r: away(r) == first, lambda g, r: to_row(g, r).wait_recv())
+        each_down(
+            lambda r: away(r) == first, lambda g, r: to_row(g, r).wait_recv(), [0, 1] + rest
+        )
 
     def scatter_x(k, s):
         for r in range(1, chips):
@@ -293,6 +301,66 @@
                 ag_x(DOWN, s, r, i).start()
             ag_c(DOWN, s, 0, i).start()
 
+    def rs_zz(s, r):
+        return remote(
+            zparts.at[s, r], recv_z.at[DOWN, s, r], rs_zz_send.at[s, r], rs_zz_recv.at[s, r],
+            {"fs": fs + 2 - 4 * zi},
+        )
+
+    def rs_zx(s, r):
+        return remote(
+            parts.at[r, 0, s, zi], recv_x.at[DOWN, r - 1, s, 0], rs_x_send.at[DOWN, s, r - 1],
+            rs_x_recv.at[DOWN, s, r - 1], {"tp": tp_of(r, c)},
+        )
+
+    def turned_z(s, rs):
+        for r in rs:
+            rs_c(DOWN, s, r).wait_recv()
+
+            def step(j, carry, r=r):
+                at = pl.ds(pl.multiple_of(j * tile, tile), tile)
+
+                def pair(i):
+                    total = parts[r, 0, s, i, at, :].astype(F32)
+                    return total + recv_core[DOWN, r, s, i, at, :].astype(F32)
+
+                zparts[s, r, at, :] = pair(other).astype(BF16)
+                parts[r, 0, s, zi, at, :] = pair(zi).astype(BF16)
+                return carry
+
+            lax.fori_loop(0, length // tile, step, 0)
+            rs_zz(s, r).start()
+
+    def turned_x(s):
+        for r in range(1, chips):
+            rs_zz(s, r).wait_recv()
+
+            def step(j, carry, r=r):
+                at = pl.ds(pl.multiple_of(j * tile, tile), tile)
+                total = parts[r, 0, s, zi, at, :].astype(F32)
+                total = total + recv_z[DOWN, s, r, at, :].astype(F32)
+                parts[r, 0, s, zi, at, :] = total.astype(BF16)
+                return carry
+
+            lax.fori_loop(0, length // tile, step, 0)
+            rs_zx(s, r).start()
+
+    def turned_finish(s):
+        rs_zz(s, 0).wait_recv()
+        for r in range(1, chips):
+            rs_zx(s, r).wait_recv()
+
+        def step(j, carry):
+            at = pl.ds(pl.multiple_of(j * tile, tile), tile)
+            total = parts[0, 0, s, zi, at, :].astype(F32)
+            total = total + recv_z[DOWN, s, 0, at, :].astype(F32)
+            for r in range(1, chips):
+                total = total + recv_x[DOWN, r - 1, s, 0, at, :].astype(F32)
+            out[s, at, :] = (xg[zi, me, s, at, :].astype(F32) + total).astype(BF16)
+            return carry
+
+        lax.fori_loop(0, length // tile, step, 0)
+
     def finish(s):
         rs_z(DOWN, s).wait_recv()
 
@@ -306,11 +374,15 @@
 
     def scatter_sent(k):
         for s in range(seqs):
+            turned = k == DOWN and s % 2
             for r in range(chips):
                 rs_c(k, s, r).wait_send()
+                if turned:
+                    rs_zz(s, r).wait_send()
                 if r:
-                    rs_x(k, s, r).wait_send()
-            rs_z(k, s).wait_send()
+                    (rs_zx(s, r) if turned else rs_x(k, s, r)).wait_send()
+            if not turned:
+                rs_z(k, s).wait_send()
 
     barrier = pltpu.get_barrier_semaphore()
     peers = [{"fs": plane(r) * 2 + y} for r in across]
@@ -494,10 +566,11 @@
     arrive(C, rest[:1])
     scatter_z(MIX, 0)
     arrive(E, rest[:1])
-    arrive(C, rest[1:])
     for s in range(1, seqs):
         scatter_z(MIX, s)
+    arrive(C, rest[1:])
     resid(0)
+    pl.when(inner == 1)(lambda: down_across(rest[:1]))
     arrive(E, rest[1:])
     gather_x(DOWN, 0)
     down_launch(True)
@@ -509,12 +582,12 @@
     complete(C)
     complete(E)
 
-    def up(s):
+    def up(s, first, count):
         def activate(gate, val):
             return gate / (1.0 + jnp.exp(-gate)) * val
 
         def step(j, carry):
-            i, t = j % 2, j // 2
+            i, t = first + j % count, j // count
             matrix = buf_c[:, :, lanes_at(t * 256, 256)].reshape(width, 256)
             both = jnp.dot(normed[s, i], matrix, preferred_element_type=F32)
             here = lanes_at((zi * second + t) * 128, 128)
@@ -523,7 +596,7 @@
             active[s, i, :, lanes_at(t * 128, 128)] = activate(gate, val).astype(BF16)
             return carry
 
-        lax.fori_loop(0, 2 * full, step, 0)
+        lax.fori_loop(0, count * full, step, 0)
         if odd:
             mid = slice(full * 128, full * 128 + 128)
             scale = join_halves(uscale[0:1, mid], uscale[1:2, mid], zi)
@@ -538,29 +611,46 @@
                 active[s, i, :, mid] = jnp.where(lanes < 64, values, 0.0).astype(BF16)
                 return carry
 
-            lax.fori_loop(0, 2, last, 0)
-
-    up(0)
-    down_arrive(True)
+            lax.fori_loop(first, first + count, last, 0)
+
+    pl.when(inner == 1)(lambda: down_across(rest[1:]))
+    up(0, 0, 2)
+    soon, late = [1] + rest[:1], rest[1:]
+    down_arrive(True, soon)
     for s in range(1, seqs):
         gather_x(DOWN, s)
         gather_done(DOWN, s)
         normalize(s, gain2)
-    down_arrive(False)
+    down_arrive(False, soon)
+    for s in range(1, seqs):
+        up(s, 0, 1)
+    down_arrive(True, late)
+    for s in range(1, seqs):
+        up(s, 1, 1)
+    down_arrive(False, late)
     scatter_sent(MIX)
     down_complete(True)
+    far = order[:-1]
     for s in range(seqs):
-        if s:
-            up(s)
-        scatter_begin(DOWN, s, order[:-1])
-        scatter_x(DOWN, s)
+        scatter_begin(DOWN, s, far)
+        if s % 2:
+            turned_z(s, far)
+        else:
+            scatter_x(DOWN, s)
     down_complete(False)
     for s in range(seqs):
         scatter_begin(DOWN, s, [0])
+        if s % 2:
+            turned_z(s, [0])
+    for s in range(0, seqs, 2):
+        scatter_z(DOWN, s)
+    for s in range(1, seqs, 2):
+        turned_x(s)
     for s in range(seqs):
-        scatter_z(DOWN, s)
-    for s in range(seqs):
-        finish(s)
+        if s % 2:
+            turned_finish(s)
+        else:
+            finish(s)
 
     gather_sent(DOWN)
     scatter_sent(DOWN)
@@ -634,10 +724,10 @@
             vmem((seqs, 2, length, sub), BF16),
             vmem((seqs, 2, length, hidden), BF16),
             vmem((chips, 2, seqs, 2, length, own), BF16),
-            vmem((seqs, 2, length, own), BF16),
+            vmem((seqs, max(2, chips), length, own), BF16),
             vmem((2, chips, seqs, 2, length, own), BF16),
             vmem((2, chips - 1, seqs, 2, length, own), BF16),
-            vmem((2, seqs, 2, length, own), BF16),
+            vmem((2, seqs, max(2, chips), length, own), BF16),
             dma((8, planes - 1)),
             dma((8, planes - 1)),
             dma((8, planes)),
@@ -650,6 +740,8 @@
             dma((2, seqs, chips, 2)),
             dma((2, seqs)),
             dma((2, seqs)),
+            dma((seqs, chips)),
+            dma((seqs, chips)),
             dma((2, seqs, chips - 1)),
             dma((2, seqs, chips - 1)),
             dma((2, seqs, chips)),

time: 234 us -> 224 us (0.957)
  Pallas kernels: 229 us -> 217 us
    pallas_call x1, Pallas kernels: 229 us -> 217 us  [on_device(): pl.pallas_call(functools.partial(layer_kernel, n, n_tp), out_shape=jax.Sh...]
where the time goes in v3:
time: 224 us; the launch traced here: 221 us
  Pallas kernels  217 us (97%)
  local copies, waits for them, and re-layouts  3.45 us (2%)
    pallas_call x1, Pallas kernels, on_device(): pl.pallas_call(functools.partial(layer_kernel, n, n_tp), out_shape=jax.Sh...  217 us

profile of v3, /device:TPU:3, one launch (start us, length us, event | category | flops | bytes accessed | tf_op | source)
XLA Modules:
  0.0 220.7 jit_solution(12096773672681585905)
XLA Ops:
  0.0 1.4 copy.17.ftaps
  1.4 217.2 %layer.1 = bf16[2,384,512]{2,1,0:T(8,128)(2,1)} custom-call(bf16[2,384,512]{2,1,0:T(8,128)(2,1)} %tok.1, f32[1,2048]{1,0:T(1,128)} %bitcast.2, f32[1,2048]{1,0:T(1,128)} %bitcast.3, f32[3,512]{1,0:T(4,128)} %iscale.1, f32[3,512]{1,0:T(4,128)} %mtaps.1, f32[2,1408]{1,0:T(2,128)} %uscale.1, f32[2,3,1408]{2,1,0:T(4,128)} %copy.17.ftaps, f32[1,256]{1,0:T(1,128)} %mscale.1, ...), custom_call_target="tpu_custom_call" | custom-call | tf_op jit(solution)/shard_map/layer/pallas_call | solution.py:703
  218.6 2.1 copy.19

commit v4 on v3

--- a/solution.py
+++ b/solution.py
@@ -15,13 +15,18 @@
 MIX, DOWN = 0, 1
 
 
-def shifted(values, by):
+def shifted(values, by, count):
+    length = values.shape[0] // count
     rows = lax.broadcasted_iota(jnp.int32, values.shape, 0)
-    return jnp.where(rows >= by, pltpu.roll(values, by, 0), 0.0)
-
-
-def causal_taps(values, taps):
-    return shifted(values, 2) * taps[0:1] + shifted(values, 1) * taps[1:2] + values * taps[2:3]
+    keep = rows >= by
+    for start in range(length, values.shape[0], length):
+        keep &= (rows < start) | (rows >= start + by)
+    return jnp.where(keep, pltpu.roll(values, by, 0), 0.0)
+
+
+def causal_taps(values, taps, count):
+    later = values * taps[2:3]
+    return shifted(values, 2, count) * taps[0:1] + shifted(values, 1, count) * taps[1:2] + later
 
 
 def join_halves(first, second, which):
@@ -180,10 +185,11 @@
             rs_c_recv.at[k, s, r], {"tp": me + 1 - 2 * c},
         )
 
-    def rs_x(k, s, r):
-        return remote(
-            parts.at[r, 0, s], recv_x.at[k, r - 1, s], rs_x_send.at[k, s, r - 1],
-            rs_x_recv.at[k, s, r - 1], {"tp": tp_of(r, c)},
+    def rs_x(k, s, r, j):
+        i = zi if j else other
+        return remote(
+            parts.at[r, 0, s, i], recv_x.at[k, r - 1, s, i], rs_x_send.at[k, s, r - 1, j],
+            rs_x_recv.at[k, s, r - 1, j], {"tp": tp_of(r, c)},
         )
 
     def rs_z(k, s):
@@ -197,13 +203,12 @@
     def products(k, s, r, side):
         owner = tp_of(r, 1 - c if side else c)
         source, held = ((gated, buf_b), (active, buf_d))[k]
-        for i in (0, 1):
-            for b in range(bpo):
-                at = owner * bpo + b
-                part = jnp.dot(source[s, i], held[at], preferred_element_type=F32)
-                parts[r, side, s, i, :, b * bw : (b + 1) * bw] = (
-                    part * buf_s[at, k : k + 1, :]
-                ).astype(BF16)
+        for b in range(bpo):
+            at = owner * bpo + b
+            lines = source[s].reshape(2 * length, source.shape[-1])
+            part = jnp.dot(lines, held[at], preferred_element_type=F32)
+            part = (part * buf_s[at, k : k + 1, :]).astype(BF16)
+            parts[r, side, s, :, :, b * bw : (b + 1) * bw] = part.reshape(2, length, bw)
 
     order = list(range(1, chips)) + [0]
     tile = 64
@@ -229,13 +234,14 @@
     def down_launch(first):
         @pl.when(away(0) == first)
         def _():
-            for r in [0, 1]:
-                launch(D, [r])
-                launch(G, [r])
+            down_across([1])
 
             @pl.when(inner == 0)
             def _():
                 down_across(rest)
+
+            if not first:
+                pl.when(inner == 1)(lambda: down_across(rest))
 
     def down_across(rs):
         for r in rs:
@@ -253,17 +259,17 @@
     def scatter_x(k, s):
         for r in range(1, chips):
             rs_c(k, s, r).wait_recv()
-
-            def step(j, carry, r=r):
-                at = pl.ds(pl.multiple_of(j * tile, tile), tile)
-                for i in (0, 1):
+            for part, i in enumerate((other, zi)):
+
+                def step(j, carry, r=r, i=i):
+                    at = pl.ds(pl.multiple_of(j * tile, tile), tile)
                     total = parts[r, 0, s, i, at, :].astype(F32)
                     total = total + recv_core[k, r, s, i, at, :].astype(F32)
                     parts[r, 0, s, i, at, :] = total.astype(BF16)
-                return carry
-
-            lax.fori_loop(0, length // tile, step, 0)
-            rs_x(k, s, r).start()
+                    return carry
+
+                lax.fori_loop(0, length // tile, step, 0)
+                rs_x(k, s, r, part).start()
 
     def quad(k, s, i, at):
         total = parts[0, 0, s, i, at, :].astype(F32) + recv_core[k, 0, s, i, at, :].astype(F32)
@@ -274,7 +280,9 @@
     def scatter_z(k, s):
         rs_c(k, s, 0).wait_recv()
         for r in range(1, chips):
-            rs_x(k, s, r).wait_recv()
+            rs_x(k, s, r, 0).wait_recv()
+            if k == MIX:
+                rs_x(k, s, r, 1).wait_recv()
 
         def step(j, carry):
             at = pl.ds(pl.multiple_of(j * tile, tile), tile)
@@ -309,8 +317,8 @@
 
     def rs_zx(s, r):
         return remote(
-            parts.at[r, 0, s, zi], recv_x.at[DOWN, r - 1, s, 0], rs_x_send.at[DOWN, s, r - 1],
-            rs_x_recv.at[DOWN, s, r - 1], {"tp": tp_of(r, c)},
+            parts.at[r, 0, s, zi], recv_x.at[DOWN, r - 1, s, 0], rs_x_send.at[DOWN, s, r - 1, 0],
+            rs_x_recv.at[DOWN, s, r - 1, 0], {"tp": tp_of(r, c)},
         )
 
     def turned_z(s, rs):
@@ -363,6 +371,8 @@
 
     def finish(s):
         rs_z(DOWN, s).wait_recv()
+        for r in range(1, chips):
+            rs_x(DOWN, s, r, 1).wait_recv()
 
         def step(j, carry):
             at = pl.ds(pl.multiple_of(j * tile, tile), tile)
@@ -379,8 +389,11 @@
                 rs_c(k, s, r).wait_send()
                 if turned:
                     rs_zz(s, r).wait_send()
-                if r:
-                    (rs_zx(s, r) if turned else rs_x(k, s, r)).wait_send()
+                if r and turned:
+                    rs_zx(s, r).wait_send()
+                elif r:
+                    for j in (0, 1):
+                        rs_x(k, s, r, j).wait_send()
             if not turned:
                 rs_z(k, s).wait_send()
 
@@ -534,6 +547,9 @@
 
     mixed = min(256, sub)
 
+    def both_of(s):
+        return normed[s].reshape(2 * length, width)
+
     def mixer(s):
         def step(j, carry):
             i, at = j % 2, j // 2 * mixed
@@ -546,7 +562,7 @@
             here = pl.ds(pl.multiple_of(zi * sub + at, 128), mixed)
             scales = iscale[:, here]
             inner = (product(1) * scales[1:2]) * (product(2) * scales[2:3])
-            convolved = causal_taps(inner, mtaps[:, here])
+            convolved = causal_taps(inner, mtaps[:, here], 1)
             cols = pl.ds(pl.multiple_of(at, 128), mixed)
             gated[s, i, :, cols] = (product(0) * scales[0:1] * convolved).astype(BF16)
             return carry
@@ -570,64 +586,60 @@
         scatter_z(MIX, s)
     arrive(C, rest[1:])
     resid(0)
-    pl.when(inner == 1)(lambda: down_across(rest[:1]))
+    pl.when((inner == 1) & away(0))(lambda: down_across(rest[:1]))
     arrive(E, rest[1:])
+    down_across([0])
     gather_x(DOWN, 0)
     down_launch(True)
     for s in range(1, seqs):
         resid(s)
-    down_launch(False)
     gather_done(DOWN, 0)
     normalize(0, gain2)
     complete(C)
     complete(E)
 
-    def up(s, first, count):
+    def up(s, first, last):
         def activate(gate, val):
             return gate / (1.0 + jnp.exp(-gate)) * val
 
-        def step(j, carry):
-            i, t = first + j % count, j // count
+        def step(t, carry):
             matrix = buf_c[:, :, lanes_at(t * 256, 256)].reshape(width, 256)
-            both = jnp.dot(normed[s, i], matrix, preferred_element_type=F32)
+            both = jnp.dot(both_of(s), matrix, preferred_element_type=F32)
             here = lanes_at((zi * second + t) * 128, 128)
-            gate = causal_taps(both[:, :128] * uscale[0:1, here], ftaps[0, :, here])
-            val = causal_taps(both[:, 128:] * uscale[1:2, here], ftaps[1, :, here])
-            active[s, i, :, lanes_at(t * 128, 128)] = activate(gate, val).astype(BF16)
+            gate = causal_taps(both[:, :128] * uscale[0:1, here], ftaps[:, 0, here], 2)
+            val = causal_taps(both[:, 128:] * uscale[1:2, here], ftaps[:, 1, here], 2)
+            values = activate(gate, val).astype(BF16)
+            active[s, :, :, lanes_at(t * 128, 128)] = values.reshape(2, length, 128)
             return carry
 
-        lax.fori_loop(0, count * full, step, 0)
-        if odd:
+        lax.fori_loop(first, last, step, 0)
+        if odd and last == full:
             mid = slice(full * 128, full * 128 + 128)
             scale = join_halves(uscale[0:1, mid], uscale[1:2, mid], zi)
-            taps = join_halves(ftaps[0, :, mid], ftaps[1, :, mid], zi)
-
-            def last(i, carry):
-                matrix = buf_c[:, :, full * 256 :].reshape(width, 128)
-                both = jnp.dot(normed[s, i], matrix, preferred_element_type=F32)
-                gate = causal_taps(both * scale, taps)
-                values = activate(gate, pltpu.roll(gate, 64, 1))
-                lanes = lax.broadcasted_iota(jnp.int32, values.shape, 1)
-                active[s, i, :, mid] = jnp.where(lanes < 64, values, 0.0).astype(BF16)
-                return carry
-
-            lax.fori_loop(first, first + count, last, 0)
-
-    pl.when(inner == 1)(lambda: down_across(rest[1:]))
-    up(0, 0, 2)
+            taps = join_halves(ftaps[:, 0, mid], ftaps[:, 1, mid], zi)
+            matrix = buf_c[:, :, full * 256 :].reshape(width, 128)
+            both = jnp.dot(both_of(s), matrix, preferred_element_type=F32)
+            gate = causal_taps(both * scale, taps, 2)
+            values = activate(gate, pltpu.roll(gate, 64, 1))
+            lanes = lax.broadcasted_iota(jnp.int32, values.shape, 1)
+            values = jnp.where(lanes < 64, values, 0.0).astype(BF16)
+            active[s, :, :, mid] = values.reshape(2, length, 128)
+
+    pl.when((inner == 1) & away(0))(lambda: down_across(rest[1:]))
+    up(0, 0, full)
+    down_launch(False)
     soon, late = [1] + rest[:1], rest[1:]
     down_arrive(True, soon)
     for s in range(1, seqs):
         gather_x(DOWN, s)
         gather_done(DOWN, s)
         normalize(s, gain2)
+    down_arrive(True, late)
+    for s in range(1, seqs):
+        up(s, 0, full // 2)
     down_arrive(False, soon)
     for s in range(1, seqs):
-        up(s, 0, 1)
-    down_arrive(True, late)
-    for s in range(1, seqs):
-        up(s, 1, 1)
-    down_arrive(False, late)
+        up(s, full // 2, full)
     scatter_sent(MIX)
     down_complete(True)
     far = order[:-1]
@@ -637,13 +649,14 @@
             turned_z(s, far)
         else:
             scatter_x(DOWN, s)
+    down_arrive(False, late)
     down_complete(False)
-    for s in range(seqs):
+    for s in range(0, seqs, 2):
         scatter_begin(DOWN, s, [0])
-        if s % 2:
-            turned_z(s, [0])
-    for s in range(0, seqs, 2):
         scatter_z(DOWN, s)
+    for s in range(1, seqs, 2):
+        scatter_begin(DOWN, s, [0])
+        turned_z(s, [0])
     for s in range(1, seqs, 2):
         turned_x(s)
     for s in range(seqs):
@@ -742,8 +755,8 @@
             dma((2, seqs)),
             dma((seqs, chips)),
             dma((seqs, chips)),
-            dma((2, seqs, chips - 1)),
-            dma((2, seqs, chips - 1)),
+            dma((2, seqs, chips - 1, 2)),
+            dma((2, seqs, chips - 1, 2)),
             dma((2, seqs, chips)),
             dma((2, seqs, chips)),
             dma((7,)),
@@ -754,7 +767,7 @@
         name="layer",
     )(
         tokens, mix_gain.reshape(1, width), ffn_gain.reshape(1, width),
-        in_scale, mix_taps, up_scale, ffn_taps, mixout_scale, down_scale, *weights,
+        in_scale, mix_taps, up_scale, ffn_taps.transpose(1, 0, 2), mixout_scale, down_scale, *weights,
     )
     return result
 

time: 224 us -> 218 us (0.973)
    pallas_call x1, Pallas kernels: 217 us -> 215 us  [on_device(): pl.pallas_call(functools.partial(layer_kernel, n, n_tp), out_shape=jax.Sh...]
where the time goes in v4:
time: 218 us; the launch traced here: 217 us
  Pallas kernels  215 us (99%)
    pallas_call x1, Pallas kernels, on_device(): pl.pallas_call(functools.partial(layer_kernel, n, n_tp), out_shape=jax.Sh...  215 us

profile of v4, /device:TPU:3, one launch (start us, length us, event | category | flops | bytes accessed | tf_op | source)
XLA Modules:
  0.0 216.7 jit_solution(12373495881801904332)
XLA Ops:
  0.0 214.6 %layer.1 = bf16[2,384,512]{2,1,0:T(8,128)(2,1)} custom-call(bf16[2,384,512]{2,1,0:T(8,128)(2,1)} %tok.1, f32[1,2048]{1,0:T(1,128)} %bitcast.4, f32[1,2048]{1,0:T(1,128)} %bitcast.5, f32[3,512]{1,0:T(4,128)} %iscale.1, f32[3,512]{1,0:T(4,128)} %mtaps.1, f32[2,1408]{1,0:T(2,128)} %uscale.1, f32[3,2,1408]{2,1,0:T(2,128)} %bitcast.3, f32[1,256]{1,0:T(1,128)} %mscale.1, ...), custom_call_target="tpu_custom_call" | custom-call | tf_op jit(solution)/shard_map/layer/pallas_call | solution.py:716
  214.6 2.1 copy.18

commit v5 on v4

--- a/solution.py
+++ b/solution.py
@@ -192,12 +192,11 @@
             rs_x_recv.at[k, s, r - 1, j], {"tp": tp_of(r, c)},
         )
 
-    def rs_z(k, s):
-        src, dst = zparts.at[s, pl.ds(0, 2)], recv_z.at[k, s, pl.ds(0, 2)]
-        if k == DOWN:
-            src, dst = zparts.at[s, other], recv_z.at[k, s, 0]
-        return remote(
-            src, dst, rs_z_send.at[k, s], rs_z_recv.at[k, s], {"fs": fs + 2 - 4 * zi},
+    def rs_z(k, s, j):
+        i = zi if j else other
+        return remote(
+            zparts.at[s, i], recv_z.at[k, s, i], rs_z_send.at[k, s, j], rs_z_recv.at[k, s, j],
+            {"fs": fs + 2 - 4 * zi},
         )
 
     def products(k, s, r, side):
@@ -223,33 +222,21 @@
     def away(r):
         return plane(r) // 2 != x
 
-    def each_down(test, do, rs):
+    def each_down(test, do, rs, groups=(D, G)):
         for r in rs:
 
             @pl.when(test(r))
             def _(r=r):
-                for g in (D, G):
+                for g in groups:
                     do(g, r)
-
-    def down_launch(first):
-        @pl.when(away(0) == first)
-        def _():
-            down_across([1])
-
-            @pl.when(inner == 0)
-            def _():
-                down_across(rest)
-
-            if not first:
-                pl.when(inner == 1)(lambda: down_across(rest))
 
     def down_across(rs):
         for r in rs:
             launch(D, [r])
             launch(G, [r])
 
-    def down_arrive(first, rs):
-        each_down(lambda r: away(r) == first, lambda g, r: arrive(g, [r]), rs)
+    def down_arrive(first, rs, groups=(D, G)):
+        each_down(lambda r: away(r) == first, lambda g, r: arrive(g, [r]), rs, groups)
 
     def down_complete(first):
         each_down(
@@ -277,37 +264,35 @@
             total = total + recv_x[k, r - 1, s, i, at, :].astype(F32)
         return total
 
-    def scatter_z(k, s):
-        rs_c(k, s, 0).wait_recv()
-        for r in range(1, chips):
-            rs_x(k, s, r, 0).wait_recv()
-            if k == MIX:
-                rs_x(k, s, r, 1).wait_recv()
-
-        def step(j, carry):
-            at = pl.ds(pl.multiple_of(j * tile, tile), tile)
-            for i in (0, 1) if k == MIX else (other,):
-                zparts[s, i, at, :] = quad(k, s, i, at).astype(BF16)
+    def scatter_z(k, s, j):
+        i = zi if j else other
+        if j == 0:
+            rs_c(k, s, 0).wait_recv()
+        for r in range(1, chips):
+            rs_x(k, s, r, j).wait_recv()
+
+        def step(line, carry):
+            at = pl.ds(pl.multiple_of(line * tile, tile), tile)
+            zparts[s, i, at, :] = quad(k, s, i, at).astype(BF16)
             return carry
 
         lax.fori_loop(0, length // tile, step, 0)
-        rs_z(k, s).start()
-
-    def resid(s):
-        rs_z(MIX, s).wait_recv()
-
-        def step(j, carry):
-            at = pl.ds(pl.multiple_of(j * tile, tile), tile)
-            for i in (0, 1):
-                total = zparts[s, i, at, :].astype(F32) + recv_z[MIX, s, i, at, :].astype(F32)
-                xg[i, me, s, at, :] = (xg[i, me, s, at, :].astype(F32) + total).astype(BF16)
+        rs_z(k, s, j).start()
+
+    def resid(s, j):
+        i = other if j else zi
+        rs_z(MIX, s, j).wait_recv()
+
+        def step(line, carry):
+            at = pl.ds(pl.multiple_of(line * tile, tile), tile)
+            total = zparts[s, i, at, :].astype(F32) + recv_z[MIX, s, i, at, :].astype(F32)
+            xg[i, me, s, at, :] = (xg[i, me, s, at, :].astype(F32) + total).astype(BF16)
             return carry
 
         lax.fori_loop(0, length // tile, step, 0)
-        for i in (0, 1):
-            for r in range(1, chips):
-                ag_x(DOWN, s, r, i).start()
-            ag_c(DOWN, s, 0, i).start()
+        for r in range(1, chips):
+            ag_x(DOWN, s, r, j).start()
+        ag_c(DOWN, s, 0, j).start()
 
     def rs_zz(s, r):
         return remote(
@@ -370,13 +355,13 @@
         lax.fori_loop(0, length // tile, step, 0)
 
     def finish(s):
-        rs_z(DOWN, s).wait_recv()
+        rs_z(DOWN, s, 0).wait_recv()
         for r in range(1, chips):
             rs_x(DOWN, s, r, 1).wait_recv()
 
         def step(j, carry):
             at = pl.ds(pl.multiple_of(j * tile, tile), tile)
-            total = quad(DOWN, s, zi, at) + recv_z[DOWN, s, 0, at, :].astype(F32)
+            total = quad(DOWN, s, zi, at) + recv_z[DOWN, s, zi, at, :].astype(F32)
             out[s, at, :] = (xg[zi, me, s, at, :].astype(F32) + total).astype(BF16)
             return carry
 
@@ -395,7 +380,8 @@
                     for j in (0, 1):
                         rs_x(k, s, r, j).wait_send()
             if not turned:
-                rs_z(k, s).wait_send()
+                for j in (0, 1) if k == MIX else (0,):
+                    rs_z(k, s, j).wait_send()
 
     barrier = pltpu.get_barrier_semaphore()
     peers = [{"fs": plane(r) * 2 + y} for r in across]
@@ -580,19 +566,25 @@
         scatter_x(MIX, s)
     arrive(E, [1])
     arrive(C, rest[:1])
-    scatter_z(MIX, 0)
+    scatter_z(MIX, 0, 0)
+    scatter_z(MIX, 0, 1)
     arrive(E, rest[:1])
     for s in range(1, seqs):
-        scatter_z(MIX, s)
+        scatter_z(MIX, s, 0)
+        scatter_z(MIX, s, 1)
+    resid(0, 0)
     arrive(C, rest[1:])
-    resid(0)
+    resid(0, 1)
     pl.when((inner == 1) & away(0))(lambda: down_across(rest[:1]))
     arrive(E, rest[1:])
     down_across([0])
     gather_x(DOWN, 0)
-    down_launch(True)
-    for s in range(1, seqs):
-        resid(s)
+    for s in range(1, seqs):
+        resid(s, 0)
+    pl.when(away(0))(lambda: down_across([1]))
+    for s in range(1, seqs):
+        resid(s, 1)
+    pl.when((inner == 0) & away(0))(lambda: down_across(rest))
     gather_done(DOWN, 0)
     normalize(0, gain2)
     complete(C)
@@ -625,21 +617,23 @@
             values = jnp.where(lanes < 64, values, 0.0).astype(BF16)
             active[s, :, :, mid] = values.reshape(2, length, 128)
 
+    up(0, 0, full // 2)
     pl.when((inner == 1) & away(0))(lambda: down_across(rest[1:]))
-    up(0, 0, full)
-    down_launch(False)
+    up(0, full // 2, full)
+    pl.when(jnp.logical_not(away(0)))(lambda: down_across([1] + rest))
     soon, late = [1] + rest[:1], rest[1:]
+    for s in range(1, seqs):
+        gather_x(DOWN, s)
     down_arrive(True, soon)
     for s in range(1, seqs):
-        gather_x(DOWN, s)
         gather_done(DOWN, s)
         normalize(s, gain2)
-    down_arrive(True, late)
-    for s in range(1, seqs):
-        up(s, 0, full // 2)
+        up(s, 0, full - full // 2)
+    down_arrive(True, late, (D,))
+    for s in range(1, seqs):
+        up(s, full - full // 2, full)
+    down_arrive(True, late, (G,))
     down_arrive(False, soon)
-    for s in range(1, seqs):
-        up(s, full // 2, full)
     scatter_sent(MIX)
     down_complete(True)
     far = order[:-1]
@@ -653,7 +647,7 @@
     down_complete(False)
     for s in range(0, seqs, 2):
         scatter_begin(DOWN, s, [0])
-        scatter_z(DOWN, s)
+        scatter_z(DOWN, s, 0)
     for s in range(1, seqs, 2):
         scatter_begin(DOWN, s, [0])
         turned_z(s, [0])
@@ -751,8 +745,8 @@
             dma((2, seqs, chips - 1, 2)),
             dma((2, seqs, chips, 2)),
             dma((2, seqs, chips, 2)),
-            dma((2, seqs)),
-            dma((2, seqs)),
+            dma((2, seqs, 2)),
+            dma((2, seqs, 2)),
             dma((seqs, chips)),
             dma((seqs, chips)),
             dma((2, seqs, chips - 1, 2)),

time: 218 us -> 214 us (0.982)
  Pallas kernels: 215 us -> 209 us
    pallas_call x1, Pallas kernels: 215 us -> 209 us  [on_device(): pl.pallas_call(functools.partial(layer_kernel, n, n_tp), out_shape=jax.Sh...]
where the time goes in v5:
time: 214 us; the launch traced here: 211 us
  Pallas kernels  209 us (98%)
    pallas_call x1, Pallas kernels, on_device(): pl.pallas_call(functools.partial(layer_kernel, n, n_tp), out_shape=jax.Sh...  209 us

profile of v5, /device:TPU:3, one launch (start us, length us, event | category | flops | bytes accessed | tf_op | source)
XLA Modules:
  0.0 211.4 jit_solution(5666996030957309419)
XLA Ops:
  0.0 209.4 %layer.1 = bf16[2,384,512]{2,1,0:T(8,128)(2,1)} custom-call(bf16[2,384,512]{2,1,0:T(8,128)(2,1)} %tok.1, f32[1,2048]{1,0:T(1,128)} %bitcast.4, f32[1,2048]{1,0:T(1,128)} %bitcast.5, f32[3,512]{1,0:T(4,128)} %iscale.1, f32[3,512]{1,0:T(4,128)} %mtaps.1, f32[2,1408]{1,0:T(2,128)} %uscale.1, f32[3,2,1408]{2,1,0:T(2,128)} %bitcast.3, f32[1,256]{1,0:T(1,128)} %mscale.1, ...), custom_call_target="tpu_custom_call" | custom-call | tf_op jit(solution)/shard_map/layer/pallas_call | solution.py:710
  209.4 2.1 copy.18

commit v6 on v5

--- a/solution.py
+++ b/solution.py
@@ -568,10 +568,11 @@
     arrive(C, rest[:1])
     scatter_z(MIX, 0, 0)
     scatter_z(MIX, 0, 1)
-    arrive(E, rest[:1])
+    pl.when(inner == 0)(lambda: arrive(E, rest[:1]))
     for s in range(1, seqs):
         scatter_z(MIX, s, 0)
         scatter_z(MIX, s, 1)
+    pl.when(inner == 1)(lambda: arrive(E, rest[:1]))
     resid(0, 0)
     arrive(C, rest[1:])
     resid(0, 1)
@@ -617,9 +618,8 @@
             values = jnp.where(lanes < 64, values, 0.0).astype(BF16)
             active[s, :, :, mid] = values.reshape(2, length, 128)
 
-    up(0, 0, full // 2)
     pl.when((inner == 1) & away(0))(lambda: down_across(rest[1:]))
-    up(0, full // 2, full)
+    up(0, 0, full)
     pl.when(jnp.logical_not(away(0)))(lambda: down_across([1] + rest))
     soon, late = [1] + rest[:1], rest[1:]
     for s in range(1, seqs):
@@ -639,6 +639,7 @@
     far = order[:-1]
     for s in range(seqs):
         scatter_begin(DOWN, s, far)
+    for s in range(seqs):
         if s % 2:
             turned_z(s, far)
         else:

time: 214 us -> 213 us (level)
  no operation moved by 1% of the time
where the time goes in v6:
time: 213 us; the launch traced here: 212 us
  Pallas kernels  210 us (99%)
    pallas_call x1, Pallas kernels, on_device(): pl.pallas_call(functools.partial(layer_kernel, n, n_tp), out_shape=jax.Sh...  210 us

profile of v6, /device:TPU:3, one launch (start us, length us, event | category | flops | bytes accessed | tf_op | source)
XLA Modules:
  0.0 212.1 jit_solution(868873080654898316)
XLA Ops:
  0.0 210.1 %layer.1 = bf16[2,384,512]{2,1,0:T(8,128)(2,1)} custom-call(bf16[2,384,512]{2,1,0:T(8,128)(2,1)} %tok.1, f32[1,2048]{1,0:T(1,128)} %bitcast.4, f32[1,2048]{1,0:T(1,128)} %bitcast.5, f32[3,512]{1,0:T(4,128)} %iscale.1, f32[3,512]{1,0:T(4,128)} %mtaps.1, f32[2,1408]{1,0:T(2,128)} %uscale.1, f32[3,2,1408]{2,1,0:T(2,128)} %bitcast.3, f32[1,256]{1,0:T(1,128)} %mscale.1, ...), custom_call_target="tpu_custom_call" | custom-call | tf_op jit(solution)/shard_map/layer/pallas_call | solution.py:711
  210.1 2.1 copy.18
